TPU v7x, 32 devices: a whole 2x2x4 slice. The times are simulated.
32 devices in a mesh: sp: 4 (over z), dp: 8 (over y, x, core).
Axes of the slice: x: 2, y: 2, z: 4, core: 2. Of those that a mesh axis runs over, the one named last changes fastest.
Arguments:
- queries: bfloat16 [8, 512, 1024], P('dp', 'sp'), may hold values from -6 to 6
- key_rows: bfloat16 [8, 512, 1024], P('dp', 'sp'), may hold values from -6 to 6
- value_rows: bfloat16 [8, 512, 1024], P('dp', 'sp'), may hold values from -6 to 6
- break_offset: bfloat16 [8, 512, 16], P('dp', 'sp'), may hold values from 1.5 to 15
- hidden_in: bfloat16 [8, 512, 2048], P('dp', 'sp'), may hold values from -6 to 6
- gate_weight: bfloat16 [2048, 1024], P('dp', 'sp'), may hold values from -0.125 to 0.125
- out_weight: bfloat16 [1024, 2048], P('sp', 'dp'), may hold values from -0.1875 to 0.1875
Outputs:
- mixed: bfloat16 [8, 512, 2048], P('dp', 'sp')
All inputs are finite; a program needn't handle non-finite values.
Results may differ from a plain program's by a relative error of at most 0.0063.
Values may be sent and summed in bfloat16 or wider, within the bound.
A program may use at most 64 MiB of HBM per device.

v0:
```python
import functools
import math
import jax
import jax.numpy as jnp
from jax import lax
from jax.experimental import pallas as pl
from jax.experimental.pallas import tpu as pltpu
from jax.sharding import PartitionSpec as P

eps_norm = 1e-05
QKV_FIRST = True


def stick_blocks(head_queries, head_keys, head_values, head_offsets):
    groups, length, head_size = head_queries.shape
    block_rows = min(512, length)
    block_count = length // block_rows
    score_scale = head_size ** (-0.5)
    query_blocks = head_queries.reshape(groups, block_count, block_rows, head_size)

    def one_block(block_index):
        query_block = lax.dynamic_index_in_dim(query_blocks, block_index, 1, keepdims=False)
        query_pos = block_index * block_rows + jnp.arange(block_rows, dtype=jnp.int32)

        def key_step(step_turn, carry):
            running, carried = carry
            key_first = (block_index - step_turn) * block_rows
            key_block = lax.dynamic_slice_in_dim(head_keys, key_first, block_rows, 1)
            value_block = lax.dynamic_slice_in_dim(head_values, key_first, block_rows, 1)
            offset_block = lax.dynamic_slice_in_dim(head_offsets, key_first, block_rows, 1)
            scores = jnp.einsum(
                "gqd,gkd->gqk", query_block, key_block, preferred_element_type=jnp.float32
            )
            scores = scores * score_scale - offset_block[:, None, :]
            key_pos = key_first + jnp.arange(block_rows, dtype=jnp.int32)
            earlier = key_pos[None, :] < query_pos[:, None]
            keep_log = jnp.where(earlier, jax.nn.log_sigmoid(-scores), 0.0)
            later_sum = lax.cumsum(keep_log, axis=2, reverse=True) - keep_log + carried
            weights = jnp.where(
                earlier, jnp.exp(jax.nn.log_sigmoid(scores) + later_sum), 0.0
            ).astype(jnp.bfloat16)
            running = running + jnp.einsum(
                "gqk,gkd->gqd", weights, value_block, preferred_element_type=jnp.float32
            )
            carried = carried + jnp.sum(keep_log, axis=2, keepdims=True)
            return (running, carried)

        start_carry = (
            jnp.zeros((groups, block_rows, head_size), jnp.float32),
            jnp.zeros((groups, block_rows, 1), jnp.float32),
        )
        running, carried = lax.fori_loop(0, block_index + 1, key_step, start_carry)
        return running

    outputs = lax.map(one_block, jnp.arange(block_count, dtype=jnp.int32))
    return outputs.transpose(1, 0, 2, 3).reshape(groups, length, head_size)


def attend(pieces):
    head_queries, head_keys, head_values, head_offsets = pieces
    item_count, length, feature_count = head_queries.shape
    heads_dev = head_offsets.shape[2]
    head_size = feature_count // heads_dev

    def split_heads(array):
        return (
            array.reshape(item_count, length, heads_dev, head_size)
            .transpose(0, 2, 1, 3)
            .reshape(item_count * heads_dev, length, head_size)
        )

    offsets = (
        head_offsets.transpose(0, 2, 1).reshape(item_count * heads_dev, length).astype(jnp.float32)
    )
    heads_out = stick_blocks(
        split_heads(head_queries), split_heads(head_keys), split_heads(head_values), offsets
    )
    mean_sq = jnp.mean(heads_out * heads_out, axis=2, keepdims=True)
    normed = (heads_out * lax.rsqrt(mean_sq + eps_norm)).astype(jnp.bfloat16)
    return (
        normed.reshape(item_count, heads_dev, length, head_size)
        .transpose(0, 2, 1, 3)
        .reshape(item_count, length, feature_count)
    )


def shards(queries, key_rows, value_rows, break_offset, hidden_in, gate_weight, out_weight):
    tokens = hidden_in[0]
    gate_rows, out_cols = (
        lax.all_gather(gate_weight, "sp", axis=1, tiled=True),
        lax.all_gather(out_weight, "sp", axis=0, tiled=True),
    )
    gate_pre = jnp.dot(
        tokens,
        lax.all_gather(gate_rows, "dp", axis=0, tiled=True),
        preferred_element_type=jnp.float32,
    )
    gate_act = jax.nn.silu(gate_pre)
    normed = attend(
        (
            lax.all_to_all(queries, "sp", split_axis=2, concat_axis=1, tiled=True),
            lax.all_to_all(key_rows, "sp", split_axis=2, concat_axis=1, tiled=True),
            lax.all_to_all(value_rows, "sp", split_axis=2, concat_axis=1, tiled=True),
            lax.all_to_all(break_offset, "sp", split_axis=2, concat_axis=1, tiled=True),
        )
    )
    returned = lax.all_to_all(normed, "sp", split_axis=1, concat_axis=2, tiled=True)
    gated_rows = (returned[0].astype(jnp.float32) * gate_act).astype(jnp.bfloat16)
    mixed_rows = jnp.dot(
        gated_rows,
        lax.all_gather(out_cols, "dp", axis=1, tiled=True),
        preferred_element_type=jnp.float32,
    )
    return mixed_rows.astype(jnp.bfloat16)[None]


log2_e = math.log2(math.e)
f32, bf16 = jnp.float32, jnp.bfloat16


def plane_kernel(
    n_sp,
    n_dp,
    head_size,
    q_ref,
    k_ref,
    v_ref,
    off_ref,
    hid_ref,
    gw_ref,
    ow_ref,
    o_ref,
    w_all,
    qh,
    kh,
    vh,
    offs,
    nout,
    ret,
    act,
    total,
    a_send,
    a_recv,
    r_send,
    r_recv,
    z_send,
    z_recv,
    x_send,
    x_recv,
    c_send,
    c_recv,
    loc_sem,
):
    s = lax.axis_index("sp")
    d = lax.axis_index("dp")
    rows = q_ref.shape[0]
    cols = q_ref.shape[1] // n_sp
    half = gw_ref.shape[0] // 2
    core, xi, yi = d % 2, (d // 2) % 2, d // 4
    d_c = d + 1 - 2 * core
    d_x = d + 2 - 4 * xi
    d_y = d + 4 - 8 * yi
    d_xy = d_x + 4 - 8 * yi
    low = s < 2
    order = [s, jnp.where(low, 1 - s, 5 - s), jnp.where(low, 2, 1), jnp.where(low, 3, 0)]
    peers = [(s + i) % n_sp for i in range(1, n_sp)]

    def cp(src, dst, ss, rs, dd, sd):
        return pltpu.make_async_remote_copy(
            src_ref=src,
            dst_ref=dst,
            send_sem=ss,
            recv_sem=rs,
            device_id=(sd, dd),
            device_id_type=pl.DeviceIdType.MESH,
        )

    local = []
    for w, ref in enumerate((gw_ref, ow_ref)):
        for hf in range(2):
            local.append(
                pltpu.make_async_copy(
                    ref.at[pl.ds(hf * half, half)], w_all.at[d, s, hf, w], loc_sem.at[2 * w + hf]
                )
            )
    mine = pl.ds(pl.multiple_of(s * cols, cols), cols)
    for i, (ref, dst) in enumerate(((q_ref, qh), (k_ref, kh), (v_ref, vh))):
        local.append(pltpu.make_async_copy(ref.at[:, mine], dst.at[s], loc_sem.at[4 + i]))
    local.append(pltpu.make_async_copy(off_ref.at[s], offs.at[s], loc_sem.at[7]))
    for c in local:
        c.start()

    barrier = pltpu.get_barrier_semaphore()
    friends = [(p, d) for p in peers] + [(s, d_x), (s, d_y), (s, d_c)]
    for ps, pd in friends:
        pl.semaphore_signal(
            barrier, inc=1, device_id=(ps, pd), device_id_type=pl.DeviceIdType.MESH
        )
    for c in local:
        c.wait()
    pl.semaphore_wait(barrier, len(friends))

    def x_copy(kind, r):
        b = order[r]
        if kind == 0:
            return cp(w_all.at[d, b], w_all.at[d, b], x_send.at[0, r], x_recv.at[0, r], d_x, s)
        if kind == 1:
            return cp(w_all.at[d, b], w_all.at[d, b], x_send.at[1, r], x_recv.at[1, r], d_y, s)
        if kind == 2:
            blk = w_all.at[d_y, b, 0]
            return cp(blk, blk, x_send.at[2, r], x_recv.at[2, r], d_x, s)
        blk = w_all.at[d_x, b, 1]
        return cp(blk, blk, x_send.at[3, r], x_recv.at[3, r], d_y, s)

    def c_copy(i, r):
        blk = w_all.at[(d, d_x, d_y, d_xy)[i], order[r]]
        return cp(blk, blk, c_send.at[i, r], c_recv.at[i, r], d_c, s)

    def z_copy(b, slot, to):
        blk = w_all.at[d, b]
        return cp(blk, blk, z_send.at[slot], z_recv.at[b], d, to)

    def z_arrival(r):
        b = order[r]
        return z_copy(b, 2 + r, s)

    def own_up_down():
        @pl.when(s < n_sp - 1)
        def _():
            z_copy(s, 0, s + 1).start()

        @pl.when(s > 0)
        def _():
            z_copy(s, 1, s - 1).start()

    middle = (s > 0) & (s < n_sp - 1)

    def forward_to(r):
        return jnp.where(order[r] < s, s + 1, s - 1)

    def stage1(r):
        if r > 0:
            z_arrival(r).wait_recv()

            @pl.when(middle)
            def _():
                z_copy(order[r], 2 + r, forward_to(r)).start()

        x_copy(0, r).start()
        x_copy(1, r).start()
        c_copy(0, r).start()

    def stage2(r):
        x_copy(1, r).wait_recv()
        x_copy(2, r).start()
        c_copy(2, r).start()
        x_copy(0, r).wait_recv()
        x_copy(3, r).start()
        c_copy(1, r).start()

    def stage3(r):
        x_copy(2, r).wait_recv()
        x_copy(3, r).wait_recv()
        c_copy(3, r).start()

    def a_copies(i):
        t = peers[i]
        theirs = pl.ds(pl.multiple_of(t * cols, cols), cols)
        out = []
        for n, (ref, dst) in enumerate(((q_ref, qh), (k_ref, kh), (v_ref, vh))):
            out.append(
                cp(ref.at[:, theirs], dst.at[s], a_send.at[n, i], a_recv.at[n, i], d, t)
            )
        out.append(cp(off_ref.at[t], offs.at[s], a_send.at[3, i], a_recv.at[3, i], d, t))
        return out

    def r_copy(i):
        t = peers[i]
        return cp(nout.at[t], ret.at[s], r_send.at[i], r_recv.at[i], d, t)

    def gate_block(r):
        b = order[r]
        for i in range(4):
            c_copy(i, r).wait_recv()

        def body(e, pre):
            lhs = hid_ref[:, pl.ds(pl.multiple_of(e * 2 * half, 2 * half), 2 * half)]
            rhs = w_all[e, b, :, 0].reshape(2 * half, cols)
            return pre + jnp.dot(lhs, rhs, preferred_element_type=f32)

        pre = lax.fori_loop(0, n_dp, body, jnp.zeros((rows, cols), f32), unroll=2)
        act[r] = pre / (1.0 + jnp.exp(-pre))

    def out_block(r):
        b = order[r]
        gated = (ret[b].astype(f32) * act[r]).astype(bf16)

        def body(e, carry):
            rhs = w_all[e, b, :, 1].reshape(cols, 2 * half)
            part = jnp.dot(gated, rhs, preferred_element_type=f32)
            if r == 0:
                total[e] = part
            elif r < n_sp - 1:
                total[e] += part
            else:
                where = pl.ds(pl.multiple_of(e * 2 * half, 2 * half), 2 * half)
                o_ref[:, where] = (total[e] + part).astype(bf16)
            return carry

        lax.fori_loop(0, n_dp, body, 0, unroll=2)

    lane = lax.broadcasted_iota(jnp.int32, (rows, 2 * head_size), 1)
    first = lane < head_size
    key_pos = lax.broadcasted_iota(jnp.int32, (rows, rows), 1)
    earlier = key_pos < lax.broadcasted_iota(jnp.int32, (rows, rows), 0)
    tri_row = lax.broadcasted_iota(jnp.int32, (2 * rows, rows), 0)
    tri_col = lax.broadcasted_iota(jnp.int32, (2 * rows, rows), 1)
    tri_row = jnp.where(tri_row >= rows, tri_row - rows, tri_row)
    tri = jnp.where(tri_row > tri_col, 1.0, 0.0).astype(bf16)

    def attend_pair(p):
        lanes = pl.ds(p * 2 * head_size, 2 * head_size)
        for i in range(n_sp):
            q_pair = qh[i, :, lanes]
            sums = []
            for h in range(2):
                q_one = jnp.where(first if h == 0 else ~first, q_pair, jnp.zeros_like(q_pair))
                carry = jnp.zeros((rows, 1), f32)
                acc = jnp.zeros((rows, 2 * head_size), f32)
                for j in range(i, -1, -1):
                    off = offs[j].astype(f32)[2 * p + h : 2 * p + h + 1, :] * log2_e
                    z = lax.dot_general(
                        q_one, kh[j, :, lanes], (((1,), (1,)), ((), ())),
                        preferred_element_type=f32,
                    )
                    z = z * (head_size ** (-0.5) * log2_e) - off
                    soft = jnp.log(1.0 + jnp.exp2(-jnp.abs(z))) * log2_e
                    keep = -(jnp.maximum(z, 0.0) + soft)
                    if j == i:
                        keep = jnp.where(earlier, keep, 0.0)
                    hi = keep.astype(bf16)
                    lo = (keep - hi.astype(f32)).astype(bf16)
                    later = jnp.dot(
                        jnp.concatenate([hi, lo], axis=1), tri, preferred_element_type=f32
                    )
                    wgt = jnp.exp2(jnp.minimum(z, 0.0) - soft + later + carry)
                    if j == i:
                        wgt = jnp.where(earlier, wgt, 0.0)
                    acc += jnp.dot(wgt.astype(bf16), vh[j, :, lanes], preferred_element_type=f32)
                    if j > 0:
                        carry += later[:, 0:1] + keep[:, 0:1]
                sums.append(acc)
            o = jnp.where(first, sums[0], sums[1])
            sq = o * o
            ms0 = jnp.sum(jnp.where(first, sq, 0.0), axis=1, keepdims=True)
            ms1 = jnp.sum(jnp.where(first, 0.0, sq), axis=1, keepdims=True)
            inv = jnp.where(
                first,
                lax.rsqrt(ms0 / head_size + eps_norm),
                lax.rsqrt(ms1 / head_size + eps_norm),
            )
            nout[i, :, lanes] = (o * inv).astype(bf16)

    pairs = cols // (2 * head_size)

    stage1(0)
    if QKV_FIRST:
        for i in range(n_sp - 1):
            for c in a_copies(i):
                c.start()
        own_up_down()
    else:
        own_up_down()
        for i in range(n_sp - 1):
            for c in a_copies(i):
                c.start()
    stage2(0)
    stage1(1)
    stage3(0)
    gate_block(0)
    stage2(1)
    for i in range(n_sp - 1):
        for c in a_copies(i):
            c.wait_recv()
    attend_pair(0)
    stage3(1)
    stage1(2)
    for p in range(1, pairs):
        attend_pair(p)
    for i in range(n_sp - 1):
        r_copy(i).start()
    ret[s] = nout[s]
    stage2(2)
    gate_block(1)
    stage1(3)
    stage3(2)
    stage2(3)
    gate_block(2)
    stage3(3)
    for i in range(n_sp - 1):
        r_copy(i).wait_recv()
    out_block(0)
    out_block(1)
    out_block(2)
    gate_block(3)
    out_block(3)

    for i in range(n_sp - 1):
        for c in a_copies(i):
            c.wait_send()
        r_copy(i).wait_send()
    for r in range(n_sp):
        for kind in range(4):
            x_copy(kind, r).wait_send()
            c_copy(kind, r).wait_send()

    @pl.when(s < n_sp - 1)
    def _():
        z_copy(s, 0, s + 1).wait_send()

    @pl.when(s > 0)
    def _():
        z_copy(s, 1, s - 1).wait_send()

    @pl.when(middle)
    def _():
        for r in range(1, n_sp):
            z_copy(order[r], 2 + r, forward_to(r)).wait_send()


def plane_shards(n_sp, n_dp, head_size, queries, key_rows, value_rows, break_offset, hidden_in, gate_weight, out_weight):
    rows, width = queries.shape[1:]
    heads_dev = break_offset.shape[2] // n_sp
    cols = width // n_sp
    depth = gate_weight.shape[0]
    offs = break_offset[0].T.reshape(n_sp, heads_dev, rows)
    vmem = pl.BlockSpec(memory_space=pltpu.VMEM)
    dma = pltpu.SemaphoreType.DMA
    mixed = pl.pallas_call(
        functools.partial(plane_kernel, n_sp, n_dp, head_size),
        out_shape=jax.ShapeDtypeStruct((rows, hidden_in.shape[2]), bf16),
        in_specs=[vmem] * 7,
        out_specs=vmem,
        scratch_shapes=[
            pltpu.VMEM((n_dp, n_sp, 2, 2, depth // 2, cols), bf16),
            pltpu.VMEM((n_sp, rows, cols), bf16),
            pltpu.VMEM((n_sp, rows, cols), bf16),
            pltpu.VMEM((n_sp, rows, cols), bf16),
            pltpu.VMEM((n_sp, heads_dev, rows), bf16),
            pltpu.VMEM((n_sp, rows, cols), bf16),
            pltpu.VMEM((n_sp, rows, cols), bf16),
            pltpu.VMEM((n_sp, rows, cols), f32),
            pltpu.VMEM((n_dp, rows, cols), f32),
            dma((4, n_sp - 1)),
            dma((4, n_sp - 1)),
            dma((n_sp - 1,)),
            dma((n_sp - 1,)),
            dma((2 + n_sp,)),
            dma((n_sp,)),
            dma((4, n_sp)),
            dma((4, n_sp)),
            dma((4, n_sp)),
            dma((4, n_sp)),
            dma((8,)),
        ],
        compiler_params=pltpu.CompilerParams(
            collective_id=0, has_side_effects=True, vmem_limit_bytes=60 * 1024 * 1024
        ),
    )(queries[0], key_rows[0], value_rows[0], offs, hidden_in[0], gate_weight, out_weight)
    return mixed[None]


def planned(mesh, shards_general):
    n_sp, n_dp = mesh.shape["sp"], mesh.shape["dp"]

    def run(*local):
        queries, break_offset, gate_weight, out_weight = local[0], local[3], local[5], local[6]
        head_size = queries.shape[2] // break_offset.shape[2]
        cols = queries.shape[2] // n_sp
        if (
            n_sp == 4
            and n_dp == 8
            and queries.shape[0] == 1
            and queries.shape[1] == 128
            and 2 * head_size == 128
            and cols % 128 == 0
            and gate_weight.shape == out_weight.shape == (cols, cols)
        ):
            return plane_shards(n_sp, n_dp, head_size, *local)
        return shards_general(*local)

    return run


def solution(mesh):
    return jax.shard_map(
        planned(mesh, shards),
        mesh=mesh,
        in_specs=(
            P("dp", "sp", None),
            P("dp", "sp", None),
            P("dp", "sp", None),
            P("dp", "sp", None),
            P("dp", "sp", None),
            P("dp", "sp"),
            P("sp", "dp"),
        ),
        out_specs=P("dp", "sp", None),
        check_vma=False,
    )
```

profile of v0, /device:TPU:0, one launch (start us, length us, event | category | flops | bytes accessed | tf_op | source)
XLA Modules:
  0.0 73.4 jit_solution(2666476666114091691)
XLA Ops:
  0.0 71.5 %shard_map.73 = bf16[128,2048]{1,0:T(8,128)(2,1)} custom-call(bf16[128,1024]{1,0:T(8,128)(2,1)} %bitcast.12, bf16[128,1024]{1,0:T(8,128)(2,1)} %bitcast.13, bf16[128,1024]{1,0:T(8,128)(2,1)} %bitcast.14, bf16[4,4,128]{2,1,0:T(4,128)(2,1)} %bitcast.15, bf16[128,2048]{1,0:T(8,128)(2,1)} %bitcast.11, bf16[256,256]{1,0:T(8,128)(2,1)} %gw_ref.1, ...), custom_call_target="tpu_custom_call" | custom-call | tf_op jit(solution)/shard_map/pallas_call | solution.py:439
  71.5 1.9 %copy.9 = bf16[1,128,2048]{2,1,0:T(8,128)(2,1)} copy(bf16[1,128,2048]{2,1,0:T(8,128)(2,1)} %bitcast.10) | data formatting | bytes 1048576
where the time goes:
time: 73.6 us; the launch traced here: 73.4 us
  Pallas kernels  71.5 us (97%)
  local copies, waits for them, and re-layouts  1.88 us (3%)
    pallas_call x1, Pallas kernels, plane_shards(): pl.pallas_call(functools.partial(plane_kernel, n_sp, n_dp, head_size), ou...  71.5 us
    unnamed x1, local copies, waits for them, and re-layouts  1.88 us

commit v1 on v0

--- a/solution.py
+++ b/solution.py
@@ -8,7 +8,6 @@
 from jax.sharding import PartitionSpec as P
 
 eps_norm = 1e-05
-QKV_FIRST = True
 
 
 def stick_blocks(head_queries, head_keys, head_values, head_offsets):
@@ -130,6 +129,7 @@
     gw_ref,
     ow_ref,
     o_ref,
+    hid,
     w_all,
     qh,
     kh,
@@ -175,19 +175,21 @@
             device_id_type=pl.DeviceIdType.MESH,
         )
 
-    local = []
+    own = []
     for w, ref in enumerate((gw_ref, ow_ref)):
         for hf in range(2):
-            local.append(
+            own.append(
                 pltpu.make_async_copy(
-                    ref.at[pl.ds(hf * half, half)], w_all.at[d, s, hf, w], loc_sem.at[2 * w + hf]
+                    ref.at[pl.ds(hf * half, half)], w_all.at[w, d, s, hf], loc_sem.at[2 * w + hf]
                 )
             )
     mine = pl.ds(pl.multiple_of(s * cols, cols), cols)
+    local = []
     for i, (ref, dst) in enumerate(((q_ref, qh), (k_ref, kh), (v_ref, vh))):
         local.append(pltpu.make_async_copy(ref.at[:, mine], dst.at[s], loc_sem.at[4 + i]))
     local.append(pltpu.make_async_copy(off_ref.at[s], offs.at[s], loc_sem.at[7]))
-    for c in local:
+    local.append(pltpu.make_async_copy(hid_ref, hid, loc_sem.at[8]))
+    for c in own + local:
         c.start()
 
     barrier = pltpu.get_barrier_semaphore()
@@ -196,96 +198,93 @@
         pl.semaphore_signal(
             barrier, inc=1, device_id=(ps, pd), device_id_type=pl.DeviceIdType.MESH
         )
-    for c in local:
+    for c in own:
         c.wait()
     pl.semaphore_wait(barrier, len(friends))
 
-    def x_copy(kind, r):
-        b = order[r]
-        if kind == 0:
-            return cp(w_all.at[d, b], w_all.at[d, b], x_send.at[0, r], x_recv.at[0, r], d_x, s)
-        if kind == 1:
-            return cp(w_all.at[d, b], w_all.at[d, b], x_send.at[1, r], x_recv.at[1, r], d_y, s)
-        if kind == 2:
-            blk = w_all.at[d_y, b, 0]
-            return cp(blk, blk, x_send.at[2, r], x_recv.at[2, r], d_x, s)
-        blk = w_all.at[d_x, b, 1]
-        return cp(blk, blk, x_send.at[3, r], x_recv.at[3, r], d_y, s)
-
-    def c_copy(i, r):
-        blk = w_all.at[(d, d_x, d_y, d_xy)[i], order[r]]
-        return cp(blk, blk, c_send.at[i, r], c_recv.at[i, r], d_c, s)
-
-    def z_copy(b, slot, to):
-        blk = w_all.at[d, b]
-        return cp(blk, blk, z_send.at[slot], z_recv.at[b], d, to)
-
-    def z_arrival(r):
-        b = order[r]
-        return z_copy(b, 2 + r, s)
-
-    def own_up_down():
+    def x_copy(kind, n):
+        w, b = n % 2, order[n // 2]
+        src = (
+            w_all.at[w, d, b],
+            w_all.at[w, d, b],
+            w_all.at[w, d_y, b, 0],
+            w_all.at[w, d_x, b, 1],
+        )[kind]
+        return cp(
+            src, src, x_send.at[kind, n], x_recv.at[kind, n], d_x if kind % 2 == 0 else d_y, s
+        )
+
+    def c_copy(i, n):
+        blk = w_all.at[n % 2, (d, d_x, d_y, d_xy)[i], order[n // 2]]
+        return cp(blk, blk, c_send.at[i, n], c_recv.at[i, n], d_c, s)
+
+    def z_copy(w, b, slot, to):
+        blk = w_all.at[w, d, b]
+        return cp(blk, blk, z_send.at[w, slot], z_recv.at[w, b], d, to)
+
+    def own_up_down(w):
         @pl.when(s < n_sp - 1)
         def _():
-            z_copy(s, 0, s + 1).start()
+            z_copy(w, s, 0, s + 1).start()
 
         @pl.when(s > 0)
         def _():
-            z_copy(s, 1, s - 1).start()
+            z_copy(w, s, 1, s - 1).start()
 
     middle = (s > 0) & (s < n_sp - 1)
 
     def forward_to(r):
         return jnp.where(order[r] < s, s + 1, s - 1)
 
-    def stage1(r):
+    def stage1(n):
+        w, r = n % 2, n // 2
         if r > 0:
-            z_arrival(r).wait_recv()
+            z_copy(w, order[r], 2 + r, s).wait_recv()
 
             @pl.when(middle)
             def _():
-                z_copy(order[r], 2 + r, forward_to(r)).start()
-
-        x_copy(0, r).start()
-        x_copy(1, r).start()
-        c_copy(0, r).start()
-
-    def stage2(r):
-        x_copy(1, r).wait_recv()
-        x_copy(2, r).start()
-        c_copy(2, r).start()
-        x_copy(0, r).wait_recv()
-        x_copy(3, r).start()
-        c_copy(1, r).start()
-
-    def stage3(r):
-        x_copy(2, r).wait_recv()
-        x_copy(3, r).wait_recv()
-        c_copy(3, r).start()
-
-    def a_copies(i):
-        t = peers[i]
+                z_copy(w, order[r], 2 + r, forward_to(r)).start()
+
+        x_copy(0, n).start()
+        x_copy(1, n).start()
+        c_copy(0, n).start()
+
+    def stage2(n):
+        x_copy(1, n).wait_recv()
+        x_copy(2, n).start()
+        c_copy(2, n).start()
+        x_copy(0, n).wait_recv()
+        x_copy(3, n).start()
+        c_copy(1, n).start()
+
+    def stage3(n):
+        x_copy(2, n).wait_recv()
+        x_copy(3, n).wait_recv()
+        c_copy(3, n).start()
+
+    def a_copies(t, source):
         theirs = pl.ds(pl.multiple_of(t * cols, cols), cols)
         out = []
         for n, (ref, dst) in enumerate(((q_ref, qh), (k_ref, kh), (v_ref, vh))):
             out.append(
-                cp(ref.at[:, theirs], dst.at[s], a_send.at[n, i], a_recv.at[n, i], d, t)
+                cp(ref.at[:, theirs], dst.at[source], a_send.at[n, t], a_recv.at[n, source], d, t)
             )
-        out.append(cp(off_ref.at[t], offs.at[s], a_send.at[3, i], a_recv.at[3, i], d, t))
+        out.append(
+            cp(off_ref.at[t], offs.at[source], a_send.at[3, t], a_recv.at[3, source], d, t)
+        )
         return out
 
-    def r_copy(i):
-        t = peers[i]
-        return cp(nout.at[t], ret.at[s], r_send.at[i], r_recv.at[i], d, t)
+    def r_copy(t, source):
+        return cp(nout.at[t], ret.at[source], r_send.at[t], r_recv.at[source], d, t)
 
     def gate_block(r):
         b = order[r]
         for i in range(4):
-            c_copy(i, r).wait_recv()
+            c_copy(i, 2 * r).wait_recv()
 
         def body(e, pre):
-            lhs = hid_ref[:, pl.ds(pl.multiple_of(e * 2 * half, 2 * half), 2 * half)]
-            rhs = w_all[e, b, :, 0].reshape(2 * half, cols)
+            lhs = hid[:, pl.ds(pl.multiple_of(e * 2 * half, 2 * half), 2 * half)]
+            rhs = w_all[0, e, b].reshape(2 * half, cols)
             return pre + jnp.dot(lhs, rhs, preferred_element_type=f32)
 
         pre = lax.fori_loop(0, n_dp, body, jnp.zeros((rows, cols), f32), unroll=2)
@@ -293,10 +292,12 @@
 
     def out_block(r):
         b = order[r]
+        for i in range(4):
+            c_copy(i, 2 * r + 1).wait_recv()
         gated = (ret[b].astype(f32) * act[r]).astype(bf16)
 
         def body(e, carry):
-            rhs = w_all[e, b, :, 1].reshape(cols, 2 * half)
+            rhs = w_all[1, e, b].reshape(cols, 2 * half)
             part = jnp.dot(gated, rhs, preferred_element_type=f32)
             if r == 0:
                 total[e] = part
@@ -318,9 +319,9 @@
     tri_row = jnp.where(tri_row >= rows, tri_row - rows, tri_row)
     tri = jnp.where(tri_row > tri_col, 1.0, 0.0).astype(bf16)
 
-    def attend_pair(p):
+    def attend(i, p):
         lanes = pl.ds(p * 2 * head_size, 2 * head_size)
-        for i in range(n_sp):
+        if True:
             q_pair = qh[i, :, lanes]
             sums = []
             for h in range(2):
@@ -363,69 +364,77 @@
 
     pairs = cols // (2 * head_size)
 
+    def attend_row(i, between):
+        @pl.when(s != i)
+        def _():
+            for c in a_copies(s, i):
+                c.wait_recv()
+
+        for p in range(pairs):
+            attend(i, p)
+            for act_on in between[p : p + 1]:
+                for stage, n in act_on:
+                    stage(n)
+
+        @pl.when(s != i)
+        def _():
+            r_copy(i, s).start()
+
+        @pl.when(s == i)
+        def _():
+            ret[i] = nout[i]
+
     stage1(0)
-    if QKV_FIRST:
-        for i in range(n_sp - 1):
-            for c in a_copies(i):
-                c.start()
-        own_up_down()
-    else:
-        own_up_down()
-        for i in range(n_sp - 1):
-            for c in a_copies(i):
-                c.start()
-    stage2(0)
+    own_up_down(0)
     stage1(1)
-    stage3(0)
-    gate_block(0)
-    stage2(1)
-    for i in range(n_sp - 1):
-        for c in a_copies(i):
-            c.wait_recv()
-    attend_pair(0)
-    stage3(1)
-    stage1(2)
-    for p in range(1, pairs):
-        attend_pair(p)
-    for i in range(n_sp - 1):
-        r_copy(i).start()
-    ret[s] = nout[s]
-    stage2(2)
-    gate_block(1)
-    stage1(3)
-    stage3(2)
-    stage2(3)
+    own_up_down(1)
+    for t in peers:
+        for c in a_copies(t, s):
+            c.start()
+    for c in local:
+        c.wait()
+    for stage, n in (
+        (stage2, 0), (stage1, 2), (stage2, 1), (stage1, 3), (stage3, 0), (stage3, 1),
+        (gate_block, 0), (stage2, 2), (stage2, 3), (stage3, 2), (gate_block, 1), (stage3, 3),
+        (stage1, 4),
+    ):
+        stage(n)
+    attend_row(0, ((), ((stage1, 5),)))
+    attend_row(1, ((), ((stage2, 4), (stage2, 5))))
+    attend_row(2, (((stage1, 6),), ((stage3, 4), (stage1, 7))))
+    attend_row(3, (((stage3, 5), (stage2, 6)), ((stage2, 7),)))
     gate_block(2)
-    stage3(3)
-    for i in range(n_sp - 1):
-        r_copy(i).wait_recv()
+    stage3(6)
+    stage3(7)
+    for t in peers:
+        r_copy(s, t).wait_recv()
     out_block(0)
     out_block(1)
     out_block(2)
     gate_block(3)
     out_block(3)
-
-    for i in range(n_sp - 1):
-        for c in a_copies(i):
+    for t in peers:
+        for c in a_copies(t, s):
             c.wait_send()
-        r_copy(i).wait_send()
-    for r in range(n_sp):
+        r_copy(t, s).wait_send()
+    for n in range(2 * n_sp):
         for kind in range(4):
-            x_copy(kind, r).wait_send()
-            c_copy(kind, r).wait_send()
-
-    @pl.when(s < n_sp - 1)
-    def _():
-        z_copy(s, 0, s + 1).wait_send()
-
-    @pl.when(s > 0)
-    def _():
-        z_copy(s, 1, s - 1).wait_send()
-
-    @pl.when(middle)
-    def _():
-        for r in range(1, n_sp):
-            z_copy(order[r], 2 + r, forward_to(r)).wait_send()
+            x_copy(kind, n).wait_send()
+            c_copy(kind, n).wait_send()
+    for w in range(2):
+
+        @pl.when(s < n_sp - 1)
+        def _():
+            z_copy(w, s, 0, s + 1).wait_send()
+
+        @pl.when(s > 0)
+        def _():
+            z_copy(w, s, 1, s - 1).wait_send()
+
+        @pl.when(middle)
+        def _():
+            for r in range(1, n_sp):
+                z_copy(w, order[r], 2 + r, forward_to(r)).wait_send()
 
 
 def plane_shards(n_sp, n_dp, head_size, queries, key_rows, value_rows, break_offset, hidden_in, gate_weight, out_weight):
@@ -438,11 +447,12 @@
     dma = pltpu.SemaphoreType.DMA
     mixed = pl.pallas_call(
         functools.partial(plane_kernel, n_sp, n_dp, head_size),
-        out_shape=jax.ShapeDtypeStruct((rows, hidden_in.shape[2]), bf16),
-        in_specs=[vmem] * 7,
+        out_shape=pltpu.VMEM((rows, hidden_in.shape[2]), bf16),
+        in_specs=[pl.BlockSpec(memory_space=pl.ANY)] * 7,
         out_specs=vmem,
         scratch_shapes=[
-            pltpu.VMEM((n_dp, n_sp, 2, 2, depth // 2, cols), bf16),
+            pltpu.VMEM((rows, depth * n_dp), bf16),
+            pltpu.VMEM((2, n_dp, n_sp, 2, depth // 2, cols), bf16),
             pltpu.VMEM((n_sp, rows, cols), bf16),
             pltpu.VMEM((n_sp, rows, cols), bf16),
             pltpu.VMEM((n_sp, rows, cols), bf16),
@@ -451,17 +461,17 @@
             pltpu.VMEM((n_sp, rows, cols), bf16),
             pltpu.VMEM((n_sp, rows, cols), f32),
             pltpu.VMEM((n_dp, rows, cols), f32),
-            dma((4, n_sp - 1)),
-            dma((4, n_sp - 1)),
-            dma((n_sp - 1,)),
-            dma((n_sp - 1,)),
-            dma((2 + n_sp,)),
-            dma((n_sp,)),
             dma((4, n_sp)),
             dma((4, n_sp)),
-            dma((4, n_sp)),
-            dma((4, n_sp)),
-            dma((8,)),
+            dma((n_sp,)),
+            dma((n_sp,)),
+            dma((2, 2 + n_sp)),
+            dma((2, n_sp)),
+            dma((4, 2 * n_sp)),
+            dma((4, 2 * n_sp)),
+            dma((4, 2 * n_sp)),
+            dma((4, 2 * n_sp)),
+            dma((9,)),
         ],
         compiler_params=pltpu.CompilerParams(
             collective_id=0, has_side_effects=True, vmem_limit_bytes=60 * 1024 * 1024

time: 73.6 us -> 58.9 us (0.80)
  Pallas kernels: 71.5 us -> 58 us
  local copies, waits for them, and re-layouts: 1.88 us -> 0.8 us
    pallas_call x1, Pallas kernels: 71.5 us -> 58 us  [plane_shards(): pl.pallas_call(functools.partial(plane_kernel, n_sp, n_dp, head_size), ou...]
    unnamed x1, local copies, waits for them, and re-layouts: 1.88 us -> 0.8 us
where the time goes in v1:
time: 58.9 us; the launch traced here: 58.8 us
  Pallas kernels  58 us (98%)
  local copies, waits for them, and re-layouts  0.8 us (1%)
    pallas_call x1, Pallas kernels, plane_shards(): pl.pallas_call(functools.partial(plane_kernel, n_sp, n_dp, head_size), ou...  58 us

profile of v1, /device:TPU:0, one launch (start us, length us, event | category | flops | bytes accessed | tf_op | source)
XLA Modules:
  0.0 58.8 jit_solution(13201221709760275791)
XLA Ops:
  0.0 58.0 %shard_map.73 = bf16[128,2048]{1,0:T(8,128)(2,1)S(1)} custom-call(bf16[128,1024]{1,0:T(8,128)(2,1)} %bitcast.12, bf16[128,1024]{1,0:T(8,128)(2,1)} %bitcast.13, bf16[128,1024]{1,0:T(8,128)(2,1)} %bitcast.14, bf16[4,4,128]{2,1,0:T(4,128)(2,1)} %bitcast.15, bf16[128,2048]{1,0:T(8,128)(2,1)} %bitcast.11, bf16[256,256]{1,0:T(8,128)(2,1)} %gw_ref.1, ...), custom_call_target="tpu_custom_call" | custom-call | tf_op jit(solution)/shard_map/pallas_call | solution.py:448
  58.0 0.8 %copy.9 = bf16[1,128,2048]{2,1,0:T(8,128)(2,1)} copy(bf16[1,128,2048]{2,1,0:T(8,128)(2,1)S(1)} %bitcast.10) | data formatting | bytes 1048576

commit v2 on v1

--- a/solution.py
+++ b/solution.py
@@ -150,6 +150,13 @@
     c_send,
     c_recv,
     loc_sem,
+    hx,
+    p_out,
+    p_in,
+    h_send,
+    h_recv,
+    p_send,
+    p_recv,
 ):
     s = lax.axis_index("sp")
     d = lax.axis_index("dp")
@@ -245,12 +252,16 @@
             def _():
                 z_copy(w, order[r], 2 + r, forward_to(r)).start()
 
-        x_copy(0, n).start()
+        if w == 1:
+            x_copy(0, n).start()
         x_copy(1, n).start()
         c_copy(0, n).start()
 
     def stage2(n):
         x_copy(1, n).wait_recv()
+        if n % 2 == 0:
+            c_copy(2, n).start()
+            return
         x_copy(2, n).start()
         c_copy(2, n).start()
         x_copy(0, n).wait_recv()
@@ -258,6 +269,8 @@
         c_copy(1, n).start()
 
     def stage3(n):
+        if n % 2 == 0:
+            return
         x_copy(2, n).wait_recv()
         x_copy(3, n).wait_recv()
         c_copy(3, n).start()
@@ -277,24 +290,41 @@
     def r_copy(t, source):
         return cp(nout.at[t], ret.at[source], r_send.at[t], r_recv.at[source], d, t)
 
+    def h_copy(yy):
+        theirs = pl.ds(pl.multiple_of((yy * 4 + (1 - xi) * 2) * 2 * half, 4 * half), 4 * half)
+        return cp(hid_ref.at[:, theirs], hx.at[yy], h_send.at[yy], h_recv.at[yy], d_x, s)
+
+    def p_copy(r):
+        return cp(p_out.at[r], p_in.at[r], p_send.at[r], p_recv.at[r], d_x, s)
+
     def gate_block(r):
         b = order[r]
-        for i in range(4):
-            c_copy(i, 2 * r).wait_recv()
-
-        def body(e, pre):
-            lhs = hid[:, pl.ds(pl.multiple_of(e * 2 * half, 2 * half), 2 * half)]
-            rhs = w_all[0, e, b].reshape(2 * half, cols)
-            return pre + jnp.dot(lhs, rhs, preferred_element_type=f32)
-
-        pre = lax.fori_loop(0, n_dp, body, jnp.zeros((rows, cols), f32), unroll=2)
-        act[r] = pre / (1.0 + jnp.exp(-pre))
+        c_copy(0, 2 * r).wait_recv()
+        c_copy(2, 2 * r).wait_recv()
+        if r == 0:
+            h_copy(0).wait_recv()
+            h_copy(1).wait_recv()
+        pre = jnp.zeros((2 * rows, cols), f32)
+        for yy in range(2):
+            for cc in range(2):
+                e = yy * 4 + xi * 2 + cc
+                lhs = hid[:, pl.ds(pl.multiple_of(e * 2 * half, 2 * half), 2 * half)]
+                other = hx[yy, :, cc * 2 * half : (cc + 1) * 2 * half]
+                rhs = w_all[0, e, b].reshape(2 * half, cols)
+                pre += jnp.dot(
+                    jnp.concatenate([lhs, other], axis=0), rhs, preferred_element_type=f32
+                )
+        act[r] = pre[:rows]
+        p_out[r] = pre[rows:].astype(bf16)
+        p_copy(r).start()
 
     def out_block(r):
         b = order[r]
         for i in range(4):
             c_copy(i, 2 * r + 1).wait_recv()
-        gated = (ret[b].astype(f32) * act[r]).astype(bf16)
+        p_copy(r).wait_recv()
+        pre = act[r] + p_in[r].astype(f32)
+        gated = (ret[b].astype(f32) * (pre / (1.0 + jnp.exp(-pre)))).astype(bf16)
 
         def body(e, carry):
             rhs = w_all[1, e, b].reshape(cols, 2 * half)
@@ -385,10 +415,12 @@
             ret[i] = nout[i]
 
     stage1(0)
+    h_copy(0).start()
+    h_copy(1).start()
     own_up_down(0)
     stage1(1)
     own_up_down(1)
-    for t in peers:
+    for t in (peers[1], peers[0], peers[2]):
         for c in a_copies(t, s):
             c.start()
     for c in local:
@@ -402,25 +434,29 @@
     attend_row(0, ((), ((stage1, 5),)))
     attend_row(1, ((), ((stage2, 4), (stage2, 5))))
     attend_row(2, (((stage1, 6),), ((stage3, 4), (stage1, 7))))
-    attend_row(3, (((stage3, 5), (stage2, 6)), ((stage2, 7),)))
-    gate_block(2)
-    stage3(6)
-    stage3(7)
+    attend_row(3, (((stage3, 5), (gate_block, 2), (stage2, 6)), ((stage2, 7),)))
+    gate_block(3)
     for t in peers:
         r_copy(s, t).wait_recv()
     out_block(0)
     out_block(1)
     out_block(2)
-    gate_block(3)
+    stage3(7)
     out_block(3)
+
     for t in peers:
         for c in a_copies(t, s):
             c.wait_send()
         r_copy(t, s).wait_send()
     for n in range(2 * n_sp):
-        for kind in range(4):
+        for kind in (1,) if n % 2 == 0 else range(4):
             x_copy(kind, n).wait_send()
+        for kind in (0, 2) if n % 2 == 0 else range(4):
             c_copy(kind, n).wait_send()
+    for r in range(n_sp):
+        p_copy(r).wait_send()
+    for yy in range(2):
+        h_copy(yy).wait_send()
     for w in range(2):
 
         @pl.when(s < n_sp - 1)
@@ -472,6 +508,13 @@
             dma((4, 2 * n_sp)),
             dma((4, 2 * n_sp)),
             dma((9,)),
+            pltpu.VMEM((2, rows, 2 * depth), bf16),
+            pltpu.VMEM((n_sp, rows, cols), bf16),
+            pltpu.VMEM((n_sp, rows, cols), bf16),
+            dma((2,)),
+            dma((2,)),
+            dma((n_sp,)),
+            dma((n_sp,)),
         ],
         compiler_params=pltpu.CompilerParams(
             collective_id=0, has_side_effects=True, vmem_limit_bytes=60 * 1024 * 1024

time: 58.9 us -> 55.5 us (0.942); the launches traced: 58.8 us -> 54.6 us
  Pallas kernels: 58 us -> 53.8 us
    pallas_call x1, Pallas kernels: 58 us -> 53.8 us  [plane_shards(): pl.pallas_call(functools.partial(plane_kernel, n_sp, n_dp, head_size), ou...]
where the time goes in v2:
time: 55.5 us; the launch traced here: 54.6 us
  Pallas kernels  53.8 us (97%)
  local copies, waits for them, and re-layouts  0.8 us (1%)
    pallas_call x1, Pallas kernels, plane_shards(): pl.pallas_call(functools.partial(plane_kernel, n_sp, n_dp, head_size), ou...  53.8 us

profile of v2, /device:TPU:0, one launch (start us, length us, event | category | flops | bytes accessed | tf_op | source)
XLA Modules:
  0.0 54.6 jit_solution(8688752431415362720)
XLA Ops:
  0.0 53.8 %shard_map.73 = bf16[128,2048]{1,0:T(8,128)(2,1)S(1)} custom-call(bf16[128,1024]{1,0:T(8,128)(2,1)} %bitcast.12, bf16[128,1024]{1,0:T(8,128)(2,1)} %bitcast.13, bf16[128,1024]{1,0:T(8,128)(2,1)} %bitcast.14, bf16[4,4,128]{2,1,0:T(4,128)(2,1)} %bitcast.15, bf16[128,2048]{1,0:T(8,128)(2,1)} %bitcast.11, bf16[256,256]{1,0:T(8,128)(2,1)} %gw_ref.1, ...), custom_call_target="tpu_custom_call" | custom-call | tf_op jit(solution)/shard_map/pallas_call | solution.py:484
  53.8 0.8 %copy.9 = bf16[1,128,2048]{2,1,0:T(8,128)(2,1)} copy(bf16[1,128,2048]{2,1,0:T(8,128)(2,1)S(1)} %bitcast.10) | data formatting | bytes 1048576
